TPU v7x, 32 devices: a whole 2x2x4 slice. The times are simulated.
32 devices in a mesh: fs: 8 (over z, x), tp: 4 (over y, core).
Axes of the slice: x: 2, y: 2, z: 4, core: 2. Of those that a mesh axis runs over, the one named last changes fastest.
Arguments:
- tokens: bfloat16 [2048, 3072], P('tp', 'fs'), may hold values from -6 to 6
- mix_gain: float32 [2048], replicated, may hold values from 0.1 to 1.9
- mlp_gain: float32 [2048], replicated, may hold values from 0.1 to 1.9
- query_weight: float32 [2048, 1024], P('fs', 'tp'), may hold values from -0.125 to 0.125
- key_weight: float32 [2048, 1024], P('fs', 'tp'), may hold values from -0.125 to 0.125
- value_weight: float32 [2048, 1024], P('fs', 'tp'), may hold values from -0.125 to 0.125
- gate_weight: float32 [2048, 1024], P('fs', 'tp'), may hold values from -0.125 to 0.125
- out_weight: float32 [1024, 2048], P('tp', 'fs'), may hold values from -0.1875 to 0.1875
- up_weight: float32 [2048, 8192], P('fs', 'tp'), may hold values from -0.125 to 0.125
- down_weight: float32 [8192, 2048], P('tp', 'fs'), may hold values from -0.0625 to 0.0625
- query_scale: float32 [1024], P(('tp', 'fs')), may hold values from 0.1 to 1.9
- key_scale: float32 [1024], P(('tp', 'fs')), may hold values from 0.1 to 1.9
- value_scale: float32 [1024], P(('tp', 'fs')), may hold values from 0.1 to 1.9
- gate_scale: float32 [1024], P(('tp', 'fs')), may hold values from 0.1 to 1.9
- out_scale: float32 [2048], P(('tp', 'fs')), may hold values from 0.1 to 1.9
- up_scale: float32 [8192], P(('tp', 'fs')), may hold values from 0.1 to 1.9
- down_scale: float32 [2048], P(('tp', 'fs')), may hold values from 0.1 to 1.9
- forget: float32 [16], P('tp'), as said below
Outputs:
- layer_out: bfloat16 [2048, 3072], P('tp', 'fs')
Inputs may be any that keep to these rules, and one draw needn't show every extreme that they name: `forget`: positive rates; each head either forgets within a few tens of positions or keeps a tenth or more over a whole sequence of 384.
All inputs are finite; a program needn't handle non-finite values.
Results may differ from a plain program's by a relative error of at most 0.02.
Values may be sent and summed in bfloat16 or wider, within the bound.
A program may use at most 64 MiB of HBM per device.

v0:
```python
import jax
import jax.numpy as jnp
from jax import lax
from jax.sharding import PartitionSpec as P


def rotary(field, pos):
    half = field.shape[-1] // 2
    inverse = 1.0 / 10000.0 ** jnp.linspace(0.0, 1.0, half, dtype=jnp.float32)
    angle = pos[:, None] * inverse[None, :]
    cosine = jnp.cos(angle)[None, :, None, :]
    sine = jnp.sin(angle)[None, :, None, :]
    paired = field.astype(jnp.float32).reshape(field.shape[:-1] + (half, 2))
    first, second = (paired[..., 0], paired[..., 1])
    turned = jnp.stack([first * cosine - second * sine, first * sine + second * cosine], axis=-1)
    return turned.reshape(field.shape)


def retain(query, key, value, gate, forget):
    batch, length, heads, width = query.shape
    block = 128
    count = length // block
    top = lax.Precision.HIGHEST
    pos = jnp.arange(length, dtype=jnp.float32)
    rot_q = rotary(query, pos)
    rot_k = rotary(key, pos) * width ** (-0.5)
    vals = value.astype(jnp.float32)
    log_decay = -forget
    steps = jnp.arange(block, dtype=jnp.float32)
    offset = steps[:, None] - steps[None, :]
    decay_mask = jnp.where(
        offset >= 0, jnp.exp(log_decay[:, None, None] * jnp.maximum(offset, 0.0)), 0.0
    )
    q_blocks = rot_q.reshape(batch, count, block, heads, width)
    k_blocks = rot_k.reshape(batch, count, block, heads, width)
    v_blocks = vals.reshape(batch, count, block, heads, width)
    inner = jnp.einsum("bnihd,bnjhd->bnhij", q_blocks, k_blocks, precision=top) * decay_mask
    inner = jnp.einsum("bnhij,bnjhe->bnihe", inner, v_blocks, precision=top)
    tail = jnp.exp(log_decay[:, None] * (block - 1.0 - steps)[None, :])
    update = jnp.einsum("bnjhd,bnjhe,hj->nbhde", k_blocks, v_blocks, tail, precision=top)
    block_decay = jnp.exp(log_decay * block)[None, :, None, None]

    def advance(state, piece):
        return (state * block_decay + piece, state)

    start_state = jnp.zeros((batch, heads, width, width), jnp.float32)
    _, before = lax.scan(advance, start_state, update)
    lead = jnp.exp(log_decay[None, :] * (steps[:, None] + 1.0))
    cross = (
        jnp.einsum("bnihd,nbhde->bnihe", q_blocks, before, precision=top)
        * lead[None, None, :, :, None]
    )
    total = inner + cross
    total = total * lax.rsqrt(jnp.mean(total * total, axis=-1, keepdims=True) + 0.01)
    total = total.reshape(batch, length, heads, width)
    return jax.nn.silu(gate.astype(jnp.float32)) * total


def norm_columns(whole, gain):
    values = whole.astype(jnp.float32)
    scale = lax.rsqrt(jnp.mean(values * values, axis=0, keepdims=True) + 1e-06)
    return (values * scale * gain[:, None]).astype(jnp.bfloat16)


def contract_first(left, right):
    return lax.dot_general(
        left, right, (((0,), (0,)), ((), ())), preferred_element_type=jnp.float32
    )


def contract_rows(weight_cols, activ):
    return lax.dot_general(
        weight_cols, activ, (((0,), (1,)), ((), ())), preferred_element_type=jnp.float32
    )


def on_device(
    tokens,
    mix_gain,
    mlp_gain,
    query_weight,
    key_weight,
    value_weight,
    gate_weight,
    out_weight,
    up_weight,
    down_weight,
    query_scale,
    key_scale,
    value_scale,
    gate_scale,
    out_scale,
    up_scale,
    down_scale,
    forget,
):
    scales = (
        lax.all_gather(query_scale, "fs", axis=0, tiled=True),
        lax.all_gather(key_scale, "fs", axis=0, tiled=True),
        lax.all_gather(value_scale, "fs", axis=0, tiled=True),
        lax.all_gather(gate_scale, "fs", axis=0, tiled=True),
        lax.all_gather(out_scale, "fs", axis=0, tiled=True),
        lax.all_gather(up_scale, "fs", axis=0, tiled=True),
        lax.all_gather(down_scale, "fs", axis=0, tiled=True),
    )
    q_scale, k_scale, v_scale, g_scale, o_scale, u_scale, d_scale = scales
    whole = lax.all_gather(tokens, "tp", axis=0, tiled=True)
    normed = norm_columns(whole, mix_gain)
    local_rows = tokens.shape[0]
    length = tokens.shape[1]
    bf_out = out_weight.astype(jnp.bfloat16)
    w_query, w_key, w_value, w_gate = (
        lax.all_gather(query_weight.astype(jnp.bfloat16), "fs", axis=0, tiled=True),
        lax.all_gather(key_weight.astype(jnp.bfloat16), "fs", axis=0, tiled=True),
        lax.all_gather(value_weight.astype(jnp.bfloat16), "fs", axis=0, tiled=True),
        lax.all_gather(gate_weight.astype(jnp.bfloat16), "fs", axis=0, tiled=True),
    )

    def project(weight, scale):
        return (contract_first(normed, weight) * scale[None, :]).astype(jnp.bfloat16)

    heads = forget.shape[0]
    shape = (1, length, heads, query_weight.shape[1] // heads)
    query = project(w_query, q_scale).reshape(shape)
    key = project(w_key, k_scale).reshape(shape)
    value = project(w_value, v_scale).reshape(shape)
    gate = project(w_gate, g_scale).reshape(shape)
    mixed_heads = retain(query, key, value, gate, forget).reshape(length, -1).astype(jnp.bfloat16)
    w_out = lax.all_gather(bf_out, "fs", axis=1, tiled=True)
    groups = lax.axis_size("tp")
    all_heads = lax.all_gather(mixed_heads, "tp", axis=1, tiled=True)
    out_rows = lax.all_to_all(w_out, "tp", split_axis=1, concat_axis=0, tiled=True)
    group = mixed_heads.shape[1]
    heads_grouped = all_heads.reshape(length, groups, group)
    rows_grouped = out_rows.reshape(groups, group, local_rows)
    parts = jnp.einsum(
        "gcf,lgc->gfl", rows_grouped, heads_grouped, preferred_element_type=jnp.float32
    )
    mix_total = jnp.sum(parts.astype(jnp.bfloat16).astype(jnp.float32), axis=0)
    after_mix = (tokens.astype(jnp.float32) + mix_total * o_scale[:, None]).astype(jnp.bfloat16)
    whole_mlp = lax.all_gather(after_mix, "tp", axis=0, tiled=True)
    normed_mlp = norm_columns(whole_mlp, mlp_gain)
    bf_up = up_weight.astype(jnp.bfloat16)
    bf_down = down_weight.astype(jnp.bfloat16)
    w_up = lax.all_gather(bf_up, "fs", axis=0, tiled=True)
    upper = contract_first(normed_mlp, w_up)
    hidden = jnp.square(jax.nn.relu(upper * u_scale[None, :])).astype(jnp.bfloat16)
    w_down = lax.all_gather(bf_down, "fs", axis=1, tiled=True)
    mlp_total = lax.psum_scatter(
        contract_rows(w_down, hidden).astype(jnp.bfloat16), "tp", scatter_dimension=0, tiled=True
    ).astype(jnp.float32)
    return (after_mix.astype(jnp.float32) + mlp_total * d_scale[:, None]).astype(jnp.bfloat16)


def solution(mesh):
    in_specs = (
        P("tp", "fs"),
        P(),
        P(),
        P("fs", "tp"),
        P("fs", "tp"),
        P("fs", "tp"),
        P("fs", "tp"),
        P("tp", "fs"),
        P("fs", "tp"),
        P("tp", "fs"),
        P(("tp", "fs")),
        P(("tp", "fs")),
        P(("tp", "fs")),
        P(("tp", "fs")),
        P(("tp", "fs")),
        P(("tp", "fs")),
        P(("tp", "fs")),
        P("tp"),
    )
    out_specs = P("tp", "fs")
    return jax.shard_map(
        on_device, mesh=mesh, in_specs=in_specs, out_specs=out_specs, check_vma=False
    )
```

profile of v0, /device:TPU:0, one launch (start us, length us, event | category | flops | bytes accessed | tf_op | source)
XLA Modules:
  0.0 579.3 jit_solution(14471361721185896337)
XLA Ops:
  6.6 1.7 copy.53
  8.4 0.7 all-gather.11.cloned.1.call-update
  9.2 1.6 convert_element_type.125
  10.9 1.6 convert_element_type.129
  12.6 1.6 convert_element_type.123
  14.3 1.6 convert_element_type.120
  16.0 1.0 copy.41
  17.0 0.6 dynamic-slice
  20.9 0.8 exponential_select_fusion
  21.7 24.3 %all-reduce.6 = (f32[256]{0:T(256)S(1)}, f32[256]{0:T(256)S(1)}, f32[256]{0:T(256)S(1)}, f32[256]{0:T(256)}, f32[512]{0:T(512)S(1)}, /*index=5*/f32[512]{0:T(512)S(1)}) all-reduce(f32[256]{0:T(256)S(1)} %dynamic-update-slice.1, f32[256]{0:T(256)S(1)} %dynamic-update-slice.3, ...), channel_id=1, replica_groups=mesh['fs'=8,'tp'=4] {'fs'}, use_global_device_ids=true, to_apply=%add.1 | all-reduce | flops 2048 | bytes 16384
  46.0 6.7 %all-gather.21.cloned.1.call-done = bf16[256,2048]{0,1:T(8,128)(2,1)} async-done(((bf16[256,256]{0,1:T(8,128)(2,1)}), bf16[256,2048]{0,1:T(8,128)(2,1)}) %all-gather.21.cloned.1.call-update) | async-done | bytes 1048592 | tf_op jit(solution)/shard_map/all_gather | solution.py:129
  52.7 2.3 copy.54
  55.0 4.2 all-to-all-start
  59.5 21.7 %all-gather.11.cloned.1.call-done = bf16[2048,384]{1,0:T(8,128)(2,1)} async-done(((bf16[512,384]{1,0:T(8,128)(2,1)}), bf16[2048,384]{1,0:T(8,128)(2,1)}) %all-gather.11.cloned.1.call-update) | async-done | bytes 1572880 | tf_op jit(solution)/shard_map/all_gather | solution.py:107
  81.2 1.8 fusion
  83.0 40.4 %all-gather.17.cloned.1.call-done = bf16[2048,256]{1,0:T(8,128)(2,1)} async-done(((bf16[256,256]{1,0:T(8,128)(2,1)}), bf16[2048,256]{1,0:T(8,128)(2,1)}) %all-gather.17.cloned.1.call-update) | async-done | bytes 1048592 | tf_op jit(solution)/shard_map/all_gather | solution.py:113
  123.4 2.7 fusion.16
  126.4 38.1 %all-gather.19.cloned.1.call-done = bf16[2048,256]{1,0:T(8,128)(2,1)} async-done(((bf16[256,256]{1,0:T(8,128)(2,1)}), bf16[2048,256]{1,0:T(8,128)(2,1)}) %all-gather.19.cloned.1.call-update) | async-done | bytes 1048592 | tf_op jit(solution)/shard_map/all_gather | solution.py:114
  164.4 2.1 fusion.18
  166.8 38.7 %all-gather.15.cloned.1.call-done = bf16[2048,256]{1,0:T(8,128)(2,1)} async-done(((bf16[256,256]{1,0:T(8,128)(2,1)}), bf16[2048,256]{1,0:T(8,128)(2,1)}) %all-gather.15.cloned.1.call-update) | async-done | bytes 1048592 | tf_op jit(solution)/shard_map/all_gather | solution.py:115
  205.4 2.2 fusion.14
  207.9 0.9 multiply_subtract_fusion.1
  208.8 0.8 pad_maximum_fusion
  209.6 0.4 mul.363
  210.1 0.7 convolution_bitcast_fusion.1
  210.9 2.3 while.13
  210.9 0.7 bitcast_dynamic-update-slice_fusion.2
  211.7 0.7 bitcast_dynamic-update-slice_fusion.2
  212.4 0.7 bitcast_dynamic-update-slice_fusion.2
  213.6 1.8 fusion.11
  215.5 2.4 convolution_multiply_fusion
  217.8 0.9 multiply_reduce_fusion
  219.1 0.5 reshape.317
  219.6 26.9 %all-gather.13.cloned.1.call-done = bf16[2048,256]{1,0:T(8,128)(2,1)} async-done(((bf16[256,256]{1,0:T(8,128)(2,1)}), bf16[2048,256]{1,0:T(8,128)(2,1)}) %all-gather.13.cloned.1.call-update) | async-done | bytes 1048592 | tf_op jit(solution)/shard_map/all_gather | solution.py:116
  246.4 2.3 multiply_convert_fusion.1
  248.7 8.9 %all_gather.60 = bf16[384,1024]{1,0:T(8,128)(2,1)S(1)} all-gather(bf16[384,256]{1,0:T(8,128)(2,1)S(1)} %multiply_convert_fusion.1), channel_id=1, replica_groups=mesh['fs'=8,'tp'=4] {'tp'}, dimensions={1}, use_global_device_ids=true | all-gather | bytes 983040 | tf_op jit(solution)/shard_map/all_gather | solution.py:131
  257.7 1.8 convert_reduce_fusion
  259.5 0.9 fusion.24
  260.5 1.1 convert_element_type.141
  261.7 2.7 convert_element_type.143
  264.5 18.3 %all-gather = f32[8,1,256]{2,1,0:T(1,128)S(1)} all-gather(f32[1,1,256]{2,1,0:T(1,128)S(1)} %bitcast.76), channel_id=1, replica_groups=mesh['fs'=8,'tp'=4] {'fs'}, dimensions={0}, use_global_device_ids=true | all-gather | bytes 9216 | tf_op jit(solution)/shard_map/all_gather | solution.py:103
  282.8 1.8 fusion.3
  284.6 120.0 %all-gather.25.cloned.1.call-done = bf16[2048,2048]{1,0:T(8,128)(2,1)} async-done(((bf16[256,2048]{1,0:T(8,128)(2,1)}), bf16[2048,2048]{1,0:T(8,128)(2,1)}) %all-gather.25.cloned.1.call-update) | async-done | bytes 8388624 | tf_op jit(solution)/shard_map/all_gather | solution.py:145
  404.7 125.2 %all-gather.27.cloned.1.call-done = bf16[2048,2048]{1,0:T(8,128)(2,1)} async-done(((bf16[2048,256]{1,0:T(8,128)(2,1)}), bf16[2048,2048]{1,0:T(8,128)(2,1)}) %all-gather.27.cloned.1.call-update) | async-done | bytes 8388624 | tf_op jit(solution)/shard_map/all_gather | solution.py:148
  529.9 14.1 %fusion.6 = bf16[2048,384]{0,1:T(8,128)(2,1)} fusion(bf16[2048,2048]{1,0:T(8,128)(2,1)} %all-gather.27.cloned.1.call-done, bf16[2048,2048]{1,0:T(8,128)(2,1)} %all-gather.25.cloned.1.call-done, bf16[2048,384]{0,1:T(8,128)(2,1)} %all-gather.23.cloned.1.call-done, f32[2048]{0:T(1024)S(1)} %bitcast.75, f32[2048]{0:T(1024)S(1)} %copy-done.8, ...), kind=kOutput, calls=%fused_computation.15 | convolution fusion | flops 6449528832 | bytes 19940864 | tf_op jit(solution)/shard_map/dot_general | solution.py:72
  544.0 26.4 %reduce-scatter.2.cloned.1.call-done = bf16[512,384]{0,1:T(8,128)(2,1)} async-done(((bf16[2048,384]{0,1:T(8,128)(2,1)}), bf16[512,384]{0,1:T(8,128)(2,1)}) %reduce-scatter.2.cloned.1.call-update) | async-done | bytes 393232 | tf_op jit(solution)/shard_map/reduce_scatter | solution.py:149
  570.4 1.1 add_convert_fusion
  571.5 0.9 copy.56
  (95 shorter events, 4.6 us)
Async XLA Ops:
  6.5 10.5 %copy-start.17 = (u32[32]{0:T(128)S(1)}, u32[32]{0:T(128)}, u32[]{:S(2)}) copy-start(u32[32]{0:T(128)} %constant.50) | copy-start | bytes 388
  6.5 9.5 %copy-start.3 = (bf16[512,384]{1,0:T(8,128)(2,1)S(1)}, bf16[512,384]{1,0:T(8,128)(2,1)}, u32[]{:S(2)}) copy-start(bf16[512,384]{1,0:T(8,128)(2,1)} %param.22) | copy-start | bytes 1179652
  6.5 12.4 %copy-start.10 = (f32[4]{0:T(128)S(1)}, f32[4]{0:T(128)}, u32[]{:S(2)}) copy-start(f32[4]{0:T(128)} %param.39) | copy-start | bytes 52
  6.5 12.9 %copy-start.11 = (f32[32]{0:T(128)S(1)}, f32[32]{0:T(128)}, u32[]{:S(2)}) copy-start(f32[32]{0:T(128)} %param.32) | copy-start | bytes 388
  6.5 13.2 %copy-start.12 = (f32[32]{0:T(128)S(1)}, f32[32]{0:T(128)}, u32[]{:S(2)}) copy-start(f32[32]{0:T(128)} %param.33) | copy-start | bytes 388
  6.5 13.4 %copy-start.13 = (f32[32]{0:T(128)S(1)}, f32[32]{0:T(128)}, u32[]{:S(2)}) copy-start(f32[32]{0:T(128)} %param.34) | copy-start | bytes 388
  6.6 13.6 %copy-start.14 = (f32[32]{0:T(128)S(1)}, f32[32]{0:T(128)}, u32[]{:S(2)}) copy-start(f32[32]{0:T(128)} %param.35) | copy-start | bytes 388
  6.6 13.8 %copy-start.15 = (f32[64]{0:T(128)S(1)}, f32[64]{0:T(128)}, u32[]{:S(2)}) copy-start(f32[64]{0:T(128)} %param.36) | copy-start | bytes 772
  6.6 14.1 %copy-start.16 = (f32[64]{0:T(128)S(1)}, f32[64]{0:T(128)}, u32[]{:S(2)}) copy-start(f32[64]{0:T(128)} %param.38) | copy-start | bytes 772
  6.6 46.1 %all-gather.21.cloned.1.call-start = ((), (), s32[]{:S(2)}) async-start(), calls=%async_computation.7 | async-start | bytes 1179648 | tf_op jit(solution)/shard_map/all_gather | solution.py:129
  8.4 72.8 %all-gather.11.cloned.1.call-start = ((), (), s32[]{:S(2)}) async-start(), calls=%async_computation.2 | async-start | bytes 1966080 | tf_op jit(solution)/shard_map/all_gather | solution.py:107
  9.1 114.3 %all-gather.17.cloned.1.call-start = ((), (), s32[]{:S(2)}) async-start(), calls=%async_computation.5 | async-start | bytes 1179648 | tf_op jit(solution)/shard_map/all_gather | solution.py:113
  10.8 153.6 %all-gather.19.cloned.1.call-start = ((), (), s32[]{:S(2)}) async-start(), calls=%async_computation.6 | async-start | bytes 1179648 | tf_op jit(solution)/shard_map/all_gather | solution.py:114
  12.5 192.9 %all-gather.15.cloned.1.call-start = ((), (), s32[]{:S(2)}) async-start(), calls=%async_computation.4 | async-start | bytes 1179648 | tf_op jit(solution)/shard_map/all_gather | solution.py:115
  14.2 232.2 %all-gather.13.cloned.1.call-start = ((), (), s32[]{:S(2)}) async-start(), calls=%async_computation.3 | async-start | bytes 1179648 | tf_op jit(solution)/shard_map/all_gather | solution.py:116
  17.0 106.4 %copy-start.6 = (f32[2048]{0:T(1024)S(1)}, f32[2048]{0:T(1024)}, u32[]{:S(2)}) copy-start(f32[2048]{0:T(1024)} %param.23) | copy-start | bytes 24580
  55.0 202.7 %all-to-all-start = ((bf16[256,4,512]{2,0,1:T(8,128)(2,1)}), bf16[256,4,512]{2,0,1:T(8,128)(2,1)}, u32[]{:S(2)}, u32[]{:S(2)}) async-start(bf16[256,4,512]{2,0,1:T(8,128)(2,1)} %copy.54), calls=%async_computation | async-start | bytes 2097152 | tf_op jit(solution)/shard_map/all_to_all | solution.py:132
  59.2 223.6 %all-gather.23.cloned.1.call-start = ((), (), s32[]{:S(2)}) async-start(), calls=%async_computation.8 | async-start | bytes 1966080 | tf_op jit(solution)/shard_map/all_gather | solution.py:141
  123.4 41.0 %copy-start.2 = (bf16[2048,384]{1,0:T(8,128)(2,1)S(1)}, bf16[2048,384]{1,0:T(8,128)(2,1)}, u32[]{:S(2)}) copy-start(bf16[2048,384]{1,0:T(8,128)(2,1)} %all-gather.11.cloned.1.call-done) | copy-start | bytes 4718596
  215.4 31.0 %copy-start.7 = (f32[2048]{0:T(1024)S(1)}, f32[2048]{0:T(1024)}, u32[]{:S(2)}) copy-start(f32[2048]{0:T(1024)} %param.23) | copy-start | bytes 24580
  215.4 31.0 %copy-start.9 = (f32[256]{0:T(256)S(1)}, f32[256]{0:T(256)}, u32[]{:S(2)}) copy-start(f32[256]{0:T(256)} %get-tuple-element.80) | copy-start | bytes 3076
  248.7 10.8 %copy-start.4 = (bf16[512,384]{0,1:T(8,128)(2,1)S(1)}, bf16[512,384]{0,1:T(8,128)(2,1)}, u32[]{:S(2)}) copy-start(bf16[512,384]{0,1:T(8,128)(2,1)} %copy.41) | copy-start | bytes 1179652
  248.7 11.8 %copy-start.1 = (f32[256,2048]{1,0:T(8,128)S(1)}, f32[256,2048]{1,0:T(8,128)}, u32[]{:S(2)}) copy-start(f32[256,2048]{1,0:T(8,128)} %param.30) | copy-start | bytes 6291460
  260.5 144.2 %all-gather.25.cloned.1.call-start = ((), (), s32[]{:S(2)}) async-start(), calls=%async_computation.9 | async-start | bytes 9437184 | tf_op jit(solution)/shard_map/all_gather | solution.py:145
  261.7 2.8 copy-start.5
  261.7 268.2 %copy-start.8 = (f32[2048]{0:T(1024)S(1)}, f32[2048]{0:T(1024)}, u32[]{:S(2)}) copy-start(f32[2048]{0:T(1024)} %param.24) | copy-start | bytes 24580
  261.7 268.2 %all-gather.27.cloned.1.call-start = ((), (), s32[]{:S(2)}) async-start(), calls=%async_computation.10 | async-start | bytes 9437184 | tf_op jit(solution)/shard_map/all_gather | solution.py:148
  264.4 306.0 %reduce-scatter.2.cloned.1.call-start = ((), (), s32[]{:S(2)}) async-start(), calls=%async_computation.11 | async-start | bytes 1966080 | tf_op jit(solution)/shard_map/reduce_scatter | solution.py:149
  529.9 40.5 %copy-start = (bf16[512,384]{0,1:T(8,128)(2,1)S(1)}, bf16[512,384]{0,1:T(8,128)(2,1)}, u32[]{:S(2)}) copy-start(bf16[512,384]{0,1:T(8,128)(2,1)} %fusion.24) | copy-start | bytes 1179652
Sparse Core Ops, SparseCore 0:
  9.5 43.1 all-gather.20
  54.3 26.8 all-gather.10
  83.3 40.0 all-gather.16
  125.4 38.9 all-gather.18
  166.4 38.9 all-gather.14
  207.4 38.9 all-gather.12
  260.6 17.4 all-gather.22
  280.2 124.4 all-gather.24
  406.7 123.1 all-gather.26
  544.2 26.1 reduce-scatter.1
where the time goes:
time: 580 us; the launch traced here: 579 us
  waiting for transfers between devices  445 us (77%)
  blocking collectives  51.5 us (9%)
  matrix products  31.1 us (5%)
  other arithmetic  21.4 us (4%)
  between operations  15.2 us (3%)
  local copies, waits for them, and re-layouts  10.2 us (2%)
    all_gather x1, waiting for transfers between devices, on_device(): w_down = lax.all_gather(bf_down, 'fs', axis=1, tiled=True)  125 us
    all_gather x1, waiting for transfers between devices, on_device(): w_up = lax.all_gather(bf_up, 'fs', axis=0, tiled=True)  120 us
    all_gather x1, waiting for transfers between devices, on_device(): lax.all_gather(query_weight.astype(jnp.bfloat16), 'fs', axis=0, tiled=True)  40.4 us
    all_gather x1, waiting for transfers between devices, on_device(): lax.all_gather(value_weight.astype(jnp.bfloat16), 'fs', axis=0, tiled=True)  38.7 us
    all_gather x1, waiting for transfers between devices, on_device(): lax.all_gather(key_weight.astype(jnp.bfloat16), 'fs', axis=0, tiled=True)  38.1 us
    all_gather x1, waiting for transfers between devices, on_device(): lax.all_gather(gate_weight.astype(jnp.bfloat16), 'fs', axis=0, tiled=True)  26.9 us
    reduce_scatter x1, waiting for transfers between devices, on_device(): lax.psum_scatter(contract_rows(w_down, hidden).astype(jnp.bfloat16), 'tp'...  26.4 us
    unnamed x1, blocking collectives  24.3 us
  transfers between devices with their start and end apart: 11, of which 9 were waited for; matrix products, arithmetic and copies ran while one was open for 7% of the time, Pallas kernels for 0%

commit v1 on v0

v1 whole, which is shorter than its diff:
```python
import functools

import jax
import jax.numpy as jnp
import numpy as np
from jax import lax
from jax.experimental import pallas as pl
from jax.experimental.pallas import tpu as pltpu
from jax.sharding import PartitionSpec as P

MESH = pl.DeviceIdType.MESH
BF = jnp.bfloat16
F32 = jnp.float32


def nn(a, b):
    return lax.dot_general(a, b, (((1,), (0,)), ((), ())), preferred_element_type=F32)


def nt(a, b):
    return lax.dot_general(a, b, (((1,), (1,)), ((), ())), preferred_element_type=F32)


def kernel(cfg, *refs):
    Z, X, n_tp, n_ch, heads = cfg
    n_fs = Z * X
    n_w = 2 + 2 * n_ch
    tok, gains, scales, cos_t, sin_t, forget = refs[:6]
    own = refs[6 : 6 + n_w]
    out_ref = refs[6 + n_w]
    rest = refs[7 + n_w :]
    full = rest[:n_w]
    (scale_g, tok_g, mix_p, mix_r, am_g, mlp_p, mlp_r, normed, proj, mixed, hidden, acc, scale_row,
     local_sem, zs, zr, xs, xr, ts, tr) = rest[n_w:]
    me = lax.axis_index("fs")
    tp = lax.axis_index("tp")
    z = me // X
    x = lax.rem(me, X)
    length, width = tok.shape
    ret = mixed.shape[1]
    head = ret // heads

    def at_z(o):
        return lax.rem(z + o, Z) * X + x

    def at_x(o):
        return z * X + lax.rem(x + o, X)

    def at_tp(o):
        return lax.rem(tp + o, n_tp)

    barrier = pltpu.get_barrier_semaphore()
    for o in range(1, Z):
        pl.semaphore_signal(barrier, inc=1, device_id={"fs": at_z(o)}, device_id_type=MESH)
    for o in range(1, X):
        pl.semaphore_signal(barrier, inc=1, device_id={"fs": at_x(o)}, device_id_type=MESH)
    for o in range(1, n_tp):
        pl.semaphore_signal(barrier, inc=1, device_id={"tp": at_tp(o)}, device_id_type=MESH)
    pl.semaphore_wait(barrier, Z - 1 + X - 1 + n_tp - 1)

    def place(w, owner):
        if w == n_w:
            return scale_g.at[owner]
        rows = own[w].shape[0]
        return full[w].at[pl.ds(pl.multiple_of(owner * rows, rows), rows)]

    def mine(w):
        return scales if w == n_w else own[w]

    pending = []

    def remote(src, dst, ss, rs, where):
        return pltpu.make_async_remote_copy(
            src_ref=src, dst_ref=dst, send_sem=ss, recv_sem=rs, device_id=where, device_id_type=MESH
        )

    def z_copy(w, o):
        return remote(mine(w), place(w, me), zs.at[w, o - 1], zr.at[w, o - 1], {"fs": at_z(o)})

    def z_send(w):
        for o in range(1, Z):
            copy = z_copy(w, o)
            copy.start()
            pending.append(copy)

    def x_own(w):
        for o in range(1, X):
            copy = remote(mine(w), place(w, me), xs.at[w, 0, o - 1], xr.at[w, 0, o - 1], {"fs": at_x(o)})
            copy.start()
            pending.append(copy)

    def relay(w):
        for k in range(1, Z):
            piece = place(w, at_z(Z - k))
            remote(mine(w), piece, zs.at[w, k - 1], zr.at[w, k - 1], {"fs": at_z(k)}).wait_recv()
            for o in range(1, X):
                copy = remote(piece, piece, xs.at[w, k, o - 1], xr.at[w, k, o - 1], {"fs": at_x(o)})
                copy.start()
                pending.append(copy)

    def finish(w):
        for k in range(Z):
            for o in range(1, X):
                owner = lax.rem(z + Z - k, Z) * X + lax.rem(x + X - o, X)
                piece = place(w, owner)
                remote(piece, piece, xs.at[w, k, o - 1], xr.at[w, k, o - 1], {"fs": at_x(o)}).wait_recv()

    def tp_copy(stage, src, dst, o):
        return remote(src, dst, ts.at[stage, o - 1], tr.at[stage, o - 1], {"tp": at_tp(o)})

    def tp_gather(stage, src, buffer):
        for o in range(1, n_tp):
            copy = tp_copy(stage, src, buffer.at[tp], o)
            copy.start()
            pending.append(copy)

    def tp_wait(stage, buffer):
        for o in range(1, n_tp):
            slot = buffer.at[at_tp(n_tp - o)]
            tp_copy(stage, slot, slot, o).wait_recv()

    def tp_scatter(stage, parts, buffer):
        for o in range(1, n_tp):
            copy = tp_copy(stage, parts.at[at_tp(o)], buffer.at[o - 1], o)
            copy.start()
            pending.append(copy)

    def tp_sum(stage, parts, buffer):
        total = parts[tp].astype(F32)
        for o in range(1, n_tp):
            tp_copy(stage, buffer.at[o - 1], buffer.at[o - 1], o).wait_recv()
            total += buffer[o - 1].astype(F32)
        return total

    def norm(buffer, row):
        square = jnp.zeros((length, 1), F32)
        for t in range(n_tp):
            v = buffer[t].astype(F32)
            square += jnp.sum(v * v, axis=-1, keepdims=True)
        factor = lax.rsqrt(square / (width * n_tp) + 1e-6)
        for t in range(n_tp):
            cols = slice(t * width, (t + 1) * width)
            normed[:, cols] = (buffer[t].astype(F32) * factor * gains[row : row + 1, cols]).astype(BF)

    ups = list(range(2, 2 + n_ch))
    downs = list(range(2 + n_ch, n_w))

    tp_gather(0, tok, tok_g)
    for w in [n_w, 0, 1]:
        z_send(w)
        x_own(w)
    for w in ups + downs:
        z_send(w)
    locals_ = [pltpu.make_async_copy(mine(w), place(w, me), local_sem.at[w]) for w in range(n_w + 1)]
    locals_.append(pltpu.make_async_copy(tok, tok_g.at[tp], local_sem.at[n_w + 1]))
    for copy in locals_:
        copy.start()
    for copy in locals_:
        copy.wait()
    tp_wait(0, tok_g)
    norm(tok_g, 0)

    relay(n_w)
    relay(0)
    x_own(ups[0])
    relay(1)
    for w in ups[1:]:
        x_own(w)
    finish(n_w)
    finish(0)
    scale = jnp.sum(scale_g[...], axis=0)
    scale_row[...] = scale
    at = 4 * ret
    out_scale = scale[:, at : at + width]
    down_scale = scale[:, at + width : at + 2 * width]
    up_at = at + 2 * width

    for i in range(4):
        piece = nn(normed[...], full[0][:, i * ret : (i + 1) * ret])
        proj[i] = (piece * scale[:, i * ret : (i + 1) * ret]).astype(BF)

    r = lax.broadcasted_iota(jnp.int32, (ret, ret), 0)
    c = lax.broadcasted_iota(jnp.int32, (ret, ret), 1)
    odd = lax.rem(c, 2) == 1
    swap = jnp.where((r == c - 1) & odd, 1.0, jnp.where((r == c + 1) & ~odd, -1.0, 0.0)).astype(BF)
    same = jnp.where(r // head == c // head, 1.0 / head, 0.0).astype(F32)

    def turn(field):
        return field.astype(F32) * cos_t[...] + nn(field, swap) * sin_t[...]

    rot_q = turn(proj[0])
    rot_k = (turn(proj[1]) * head ** (-0.5)).astype(BF)
    vals = proj[2]
    rows = lax.broadcasted_iota(jnp.int32, (length, length), 0)
    cols = lax.broadcasted_iota(jnp.int32, (length, length), 1)
    dist = (rows - cols).astype(F32)
    lane = lax.broadcasted_iota(jnp.int32, (length, ret), 1) // head
    total = jnp.zeros((length, ret), F32)
    for h in range(heads):
        q_h = jnp.where(lane == h, rot_q, 0.0).astype(BF)
        decay = jnp.where(dist >= 0.0, jnp.exp(-forget[h] * jnp.maximum(dist, 0.0)), 0.0)
        inner = (nt(q_h, rot_k) * decay).astype(BF)
        total = jnp.where(lane == h, nn(inner, vals), total)
    mean = lax.dot_general(
        total * total, same, (((1,), (0,)), ((), ())), precision=lax.Precision.HIGHEST, preferred_element_type=F32
    )
    gate = proj[3].astype(F32)
    mixed[...] = (gate / (1.0 + jnp.exp(-gate)) * (total * lax.rsqrt(mean + 0.01))).astype(BF)

    finish(1)
    for t in range(n_tp):
        mix_p[t] = nt(mixed[...], full[1][t * width : (t + 1) * width, :]).astype(BF)
    tp_scatter(1, mix_p, mix_r)
    relay(ups[0])
    after = (tok[...].astype(F32) + tp_sum(1, mix_p, mix_r) * out_scale).astype(BF)
    am_g[tp] = after
    tp_gather(2, am_g.at[tp], am_g)
    x_own(downs[0])
    relay(ups[1])
    tp_wait(2, am_g)
    norm(am_g, 1)

    chain = ups + downs
    for w in downs[1:]:
        x_own(w)
    for i, w in enumerate(chain):
        if i + 1 < len(chain) and i + 1 > 1:
            relay(chain[i + 1])
        finish(w)
        if i < n_ch:
            size = full[w].shape[1]
            step = size // max(1, size // 256)

            def up_tile(j, carry, w=w, i=i, size=size, step=step):
                here = pl.ds(pl.multiple_of(j * step, step), step)
                u = nn(normed[...], full[w][:, here])
                s = scale_row[:, pl.ds(pl.multiple_of(up_at + i * size + j * step, 128), step)]
                u = jnp.maximum(u * s, 0.0)
                hidden[i, :, here] = (u * u).astype(BF)
                return carry

            lax.fori_loop(0, size // step, up_tile, 0)
        else:
            k = i - n_ch

            def down_tile(t, carry, w=w, k=k):
                part = nt(hidden[k], full[w][pl.ds(pl.multiple_of(t * width, width), width), :])
                if k:
                    part = part + acc[t]
                if k < n_ch - 1:
                    acc[t] = part
                else:
                    mlp_p[t] = part.astype(BF)
                return carry

            lax.fori_loop(0, n_tp, down_tile, 0)
    tp_scatter(3, mlp_p, mlp_r)
    out_ref[...] = (am_g[tp].astype(F32) + tp_sum(3, mlp_p, mlp_r) * down_scale).astype(BF)
    for copy in pending:
        copy.wait_send()


def tables(length, head, heads):
    half = head // 2
    inverse = 1.0 / 10000.0 ** np.linspace(0.0, 1.0, half)
    angle = np.arange(length)[:, None] * inverse.astype(np.float32).astype(np.float64)[None, :]
    spread = lambda a: np.tile(np.repeat(a, 2, axis=1), (1, heads)).astype(np.float32)
    return spread(np.cos(angle)), spread(np.sin(angle))


def solution(mesh):
    n_fs, n_tp = mesh.shape["fs"], mesh.shape["tp"]
    heights = [getattr(d, "coords", (0, 0, i))[2] for i, d in enumerate(mesh.devices[:, 0])]
    X = heights.count(heights[0])
    if n_fs % X:
        X = 1
    Z = n_fs // X

    def on_device(tokens, mix_gain, mlp_gain, wq, wk, wv, wg, wo, wu, wd, sq, sk, sv, sg, so, su, sd, forget):
        width, length = tokens.shape
        D = width * n_tp
        ret = wq.shape[1]
        heads = forget.shape[0]
        ff = wu.shape[1]
        n_ch = 4 if ff % 512 == 0 else 1
        chunk = ff // n_ch
        me = lax.axis_index("fs")

        def spot(s):
            wide = jnp.tile(s, n_fs)
            return jnp.where(jnp.arange(wide.shape[0]) // s.shape[0] == me, wide, 0.0)

        scales = jnp.concatenate([spot(s) for s in (sq, sk, sv, sg, so, sd, su)])[None, :]
        gains = jnp.stack([mix_gain, mlp_gain])
        cos_t, sin_t = tables(length, ret // heads, heads)
        own = [jnp.concatenate([w.astype(BF) for w in (wq, wk, wv, wg)], axis=1), wo.astype(BF).T]
        own += [wu[:, i * chunk : (i + 1) * chunk].astype(BF) for i in range(n_ch)]
        own += [wd[i * chunk : (i + 1) * chunk].astype(BF).T for i in range(n_ch)]
        n_w = len(own)
        vm = pl.BlockSpec(memory_space=pltpu.VMEM)
        block = (n_tp, length, width)
        dma = pltpu.SemaphoreType.DMA
        scratch = [pltpu.VMEM((n_fs * w.shape[0], w.shape[1]), BF) for w in own]
        scratch += [
            pltpu.VMEM((n_fs,) + scales.shape, F32),
            pltpu.VMEM(block, BF),
            pltpu.VMEM(block, BF),
            pltpu.VMEM((n_tp - 1,) + block[1:], BF),
            pltpu.VMEM(block, BF),
            pltpu.VMEM(block, BF),
            pltpu.VMEM((n_tp - 1,) + block[1:], BF),
            pltpu.VMEM((length, D), BF),
            pltpu.VMEM((4, length, ret), BF),
            pltpu.VMEM((length, ret), BF),
            pltpu.VMEM((n_ch, length, chunk), BF),
            pltpu.VMEM(block, F32),
            pltpu.VMEM(scales.shape, F32),
            dma((n_w + 2,)),
            dma((n_w + 1, Z - 1)),
            dma((n_w + 1, Z - 1)),
            dma((n_w + 1, Z, X - 1)),
            dma((n_w + 1, Z, X - 1)),
            dma((4, n_tp - 1)),
            dma((4, n_tp - 1)),
        ]
        out = pl.pallas_call(
            functools.partial(kernel, (Z, X, n_tp, n_ch, heads)),
            out_shape=jax.ShapeDtypeStruct((length, width), BF),
            in_specs=[vm] * 5 + [pl.BlockSpec(memory_space=pltpu.SMEM)] + [vm] * n_w,
            out_specs=vm,
            scratch_shapes=scratch,
            compiler_params=pltpu.CompilerParams(
                collective_id=0, has_side_effects=True, vmem_limit_bytes=60 * 2**20
            ),
            name="layer",
        )(tokens.T, gains, scales, jnp.asarray(cos_t), jnp.asarray(sin_t), forget, *own)
        return out.T

    cut = P(("tp", "fs"))
    rows, cols = P("fs", "tp"), P("tp", "fs")
    in_specs = (cols, P(), P(), rows, rows, rows, rows, cols, rows, cols) + (cut,) * 7 + (P("tp"),)
    return jax.shard_map(on_device, mesh=mesh, in_specs=in_specs, out_specs=cols, check_vma=False)
```

time: 580 us -> 327 us (0.56)
  the two profiles are of different devices: /device:TPU:0 before, /device:TPU:9 now
where the time goes in v1:
time: 327 us; the launch traced here: 326 us
  Pallas kernels  312 us (95%)
  local copies, waits for them, and re-layouts  11.1 us (3%)
  other arithmetic  3.5 us (1%)
    pallas_call x1, Pallas kernels, on_device(): pl.pallas_call(functools.partial(kernel, (Z, X, n_tp, n_ch, heads)), out_...  312 us

profile of v1, /device:TPU:9, one launch (start us, length us, event | category | flops | bytes accessed | tf_op | source)
XLA Modules:
  0.0 326.3 jit_solution(9493963023809708337)
XLA Ops:
  0.0 0.0 copy-start
  0.0 0.7 tile.28
  0.7 0.1 tile.29
  0.8 0.7 tile.30
  1.4 0.1 tile.31
  1.5 0.7 tile.32
  2.2 0.1 tile.33
  2.3 0.7 tile.34
  2.9 0.1 tile.70
  3.0 0.7 tile.71
  3.7 0.1 tile.72
  3.8 0.7 tile.73
  4.4 0.1 tile.74
  4.5 0.0 copy-done
  4.5 0.0 copy-start.8
  4.5 0.0 copy-start.1
  4.6 1.9 convert.12
  6.4 1.0 fusion.9
  7.5 0.0 copy-done.8
  7.5 0.0 copy-done.1
  7.5 0.0 copy-start.3
  7.5 0.6 copy.23
  8.1 0.0 copy-start.4
  8.1 0.0 copy-start.5
  8.1 0.0 copy-start.6
  8.1 0.0 copy-start.2
  8.1 1.0 slice_bitcast_fusion
  9.1 0.0 copy-start.7
  9.1 0.0 copy-start.9
  9.1 0.0 copy-start.10
  9.1 0.0 copy-done.3
  9.2 0.0 copy-done.4
  9.2 0.1 copy-done.5
  9.3 0.2 copy-done.6
  9.6 0.9 pad_maximum_fusion.refs_6_
  10.5 0.0 copy-done.2
  10.5 0.9 copy.21
  11.4 0.0 copy-done.7
  11.4 0.8 copy.22
  12.2 0.0 copy-done.9
  12.2 0.0 copy-done.10
  12.2 0.6 pad_maximum_fusion.1.refs_1_
  12.8 311.5 %layer.1 = bf16[384,512]{1,0:T(8,128)(2,1)} custom-call(bf16[384,512]{1,0:T(8,128)(2,1)} %bitcast.20, f32[2,2048]{1,0:T(2,128)} %pad_maximum_fusion.1.refs_1_, f32[1,4096]{1,0:T(1,128)} %bitcast.23, f32[384,256]{1,0:T(8,128)} %constant.68.clone.refs_3_, f32[384,256]{1,0:T(8,128)} %constant.69.clone.refs_4_, f32[4]{0:T(128)} %refs_5_.1, ...), custom_call_target="tpu_custom_call" | custom-call | tf_op jit(solution)/shard_map/layer/pallas_call | solution.py:326
  324.3 1.9 copy.24
  (14 shorter events, 0.1 us)
Async XLA Ops:
  0.0 4.5 %copy-start = (f32[256]{0:T(256)S(1)}, f32[256]{0:T(256)}, u32[]{:S(2)}) copy-start(f32[256]{0:T(256)} %param.35) | copy-start | bytes 3076
  4.5 2.9 copy-start.8
  4.5 2.9 copy-start.1
  7.5 1.7 copy-start.3
  8.1 1.1 copy-start.4
  8.1 1.2 copy-start.5
  8.1 1.5 copy-start.6
  8.1 2.4 copy-start.2
  9.1 2.3 copy-start.7
  9.1 3.1 copy-start.9
  9.1 3.1 copy-start.10

commit v2 on v1

v2 whole, which is shorter than its diff:
```python
import functools

import jax
import jax.numpy as jnp
import numpy as np
from jax import lax
from jax.experimental import pallas as pl
from jax.experimental.pallas import tpu as pltpu
from jax.sharding import PartitionSpec as P

MESH = pl.DeviceIdType.MESH
BF = jnp.bfloat16
F32 = jnp.float32


def nn(a, b):
    return lax.dot_general(a, b, (((1,), (0,)), ((), ())), preferred_element_type=F32)


def nt(a, b):
    return lax.dot_general(a, b, (((1,), (1,)), ((), ())), preferred_element_type=F32)


def kernel(cfg, *refs):
    Z, X, Y, C, heads = cfg
    n_tp = Y * C
    n_w = 4
    tok, gains, scales, cos_t, sin_t, forget = refs[:6]
    own = refs[6 : 6 + n_w]
    out_ref = refs[6 + n_w]
    rest = refs[7 + n_w :]
    full = rest[:n_w]
    (scale_g, scale_row, tok_g, seqs, parts, core_in, y_out, y_in, z_out, z_in, normed, proj, mixed, hidden,
     local_sem, zs, zr, xs, xr, ts, tr, azs, azr, ays, ayr, acs, acr, rcs, rcr, rys, ryr, rzs, rzr) = rest[n_w:]
    me = lax.axis_index("fs")
    tp = lax.axis_index("tp")
    z = me // X
    x = lax.rem(me, X)
    y = tp // C
    core = lax.rem(tp, C)
    length, width = tok.shape
    ret = mixed.shape[1]
    head = ret // heads

    def at_z(o):
        return lax.rem(z + o, Z) * X + x

    def at_x(o):
        return z * X + lax.rem(x + o, X)

    def at_tp(o):
        return lax.rem(tp + o, n_tp)

    def at_y(o):
        return lax.rem(y + o, Y) * C + core

    def at_core(o):
        return y * C + lax.rem(core + o, C)

    barrier = pltpu.get_barrier_semaphore()
    for o in range(1, Z):
        pl.semaphore_signal(barrier, inc=1, device_id={"fs": at_z(o)}, device_id_type=MESH)
    for o in range(1, X):
        pl.semaphore_signal(barrier, inc=1, device_id={"fs": at_x(o)}, device_id_type=MESH)
    for o in range(1, n_tp):
        pl.semaphore_signal(barrier, inc=1, device_id={"tp": at_tp(o)}, device_id_type=MESH)
    pl.semaphore_wait(barrier, Z - 1 + X - 1 + n_tp - 1)

    pending = []

    def remote(src, dst, ss, rs, where):
        return pltpu.make_async_remote_copy(
            src_ref=src, dst_ref=dst, send_sem=ss, recv_sem=rs, device_id=where, device_id_type=MESH
        )

    def send(*parts_of):
        copy = remote(*parts_of)
        copy.start()
        pending.append(copy)

    def place(w, owner):
        if w == n_w:
            return scale_g.at[owner]
        rows = own[w].shape[-2]
        return full[w].at[pl.ds(pl.multiple_of(owner * rows, rows), rows)]

    def mine(w, o):
        if w == n_w:
            return scales
        return own[w].at[lax.rem(z + o, Z)] if w >= 2 else own[w]

    def z_send(w):
        for o in range(1, Z):
            send(mine(w, o), place(w, me), zs.at[w, o - 1], zr.at[w, o - 1], {"fs": at_z(o)})

    def x_own(w):
        for o in range(1, X):
            send(mine(w, 0), place(w, me), xs.at[w, 0, o - 1], xr.at[w, 0, o - 1], {"fs": at_x(o)})

    def relay(w):
        for k in range(1, Z):
            piece = place(w, at_z(Z - k))
            remote(piece, piece, zs.at[w, k - 1], zr.at[w, k - 1], {"fs": at_z(k)}).wait_recv()
            for o in range(1, X):
                send(piece, piece, xs.at[w, k, o - 1], xr.at[w, k, o - 1], {"fs": at_x(o)})

    def finish(w):
        for k in range(Z):
            for o in range(1, X):
                owner = lax.rem(z + Z - k, Z) * X + lax.rem(x + X - o, X)
                piece = place(w, owner)
                remote(piece, piece, xs.at[w, k, o - 1], xr.at[w, k, o - 1], {"fs": at_x(o)}).wait_recv()

    def store_parts(k, t, value):
        parts[k, t % C, t // C] = value.astype(BF)

    def reduce_start(k):
        for o in range(1, C):
            send(parts.at[k, lax.rem(core + o, C)], core_in.at[k, o - 1], rcs.at[k, o - 1], rcr.at[k, o - 1],
                 {"tp": at_core(o)})

    def reduce_core(k):
        for o in range(1, C):
            slot = core_in.at[k, o - 1]
            remote(slot, slot, rcs.at[k, o - 1], rcr.at[k, o - 1], {"tp": at_core(o)}).wait_recv()
        for j in range(Y):
            value = parts[k, core, j].astype(F32)
            for o in range(1, C):
                value += core_in[k, o - 1, j].astype(F32)
            y_out[k, j] = value.astype(BF)
        for j in range(1, Y):
            send(y_out.at[k, lax.rem(y + j, Y)], y_in.at[k, j - 1], rys.at[k, j - 1], ryr.at[k, j - 1],
                 {"tp": at_y(j)})

    def reduce_y(k):
        value = y_out[k, y].astype(F32)
        for j in range(1, Y):
            slot = y_in.at[k, j - 1]
            remote(slot, slot, rys.at[k, j - 1], ryr.at[k, j - 1], {"tp": at_y(j)}).wait_recv()
            value += y_in[k, j - 1].astype(F32)
        return value

    def norm(block, row):
        square = jnp.zeros((length, 1), F32)
        for t in range(n_tp):
            v = block(t)[...].astype(F32)
            square += jnp.sum(v * v, axis=-1, keepdims=True)
        factor = lax.rsqrt(square / (width * n_tp) + 1e-6)
        for t in range(n_tp):
            cols = slice(t * width, (t + 1) * width)
            normed[:, cols] = (block(t)[...].astype(F32) * factor * gains[row : row + 1, cols]).astype(BF)

    for o in range(1, n_tp):
        send(tok, tok_g.at[tp], ts.at[o - 1], tr.at[o - 1], {"tp": at_tp(o)})
    for w in (n_w, 0, 1):
        z_send(w)
        x_own(w)
    z_send(2)
    z_send(3)
    locals_ = [pltpu.make_async_copy(mine(w, 0), place(w, me), local_sem.at[w]) for w in range(n_w + 1)]
    locals_.append(pltpu.make_async_copy(tok, tok_g.at[tp], local_sem.at[n_w + 1]))
    for copy in locals_:
        copy.start()
    for copy in locals_:
        copy.wait()
    for o in range(1, n_tp):
        slot = tok_g.at[at_tp(n_tp - o)]
        remote(slot, slot, ts.at[o - 1], tr.at[o - 1], {"tp": at_tp(o)}).wait_recv()
    norm(lambda t: tok_g.at[t], 0)

    relay(n_w)
    relay(0)
    relay(1)
    x_own(2)
    x_own(3)
    finish(n_w)
    finish(0)
    scale = jnp.sum(scale_g[...], axis=0)
    scale_row[...] = scale
    at = 4 * ret
    out_scale = scale[:, at : at + width]
    down_scale = scale[:, at + width : at + 2 * width]
    up_at = at + 2 * width

    for i in range(4):
        piece = nn(normed[...], full[0][:, i * ret : (i + 1) * ret])
        proj[i] = (piece * scale[:, i * ret : (i + 1) * ret]).astype(BF)

    r = lax.broadcasted_iota(jnp.int32, (ret, ret), 0)
    c = lax.broadcasted_iota(jnp.int32, (ret, ret), 1)
    odd = lax.rem(c, 2) == 1
    swap = jnp.where((r == c - 1) & odd, 1.0, jnp.where((r == c + 1) & ~odd, -1.0, 0.0)).astype(BF)
    same = jnp.where(r // head == c // head, 1.0 / head, 0.0).astype(F32)

    def turn(field):
        return field.astype(F32) * cos_t[...] + nn(field, swap) * sin_t[...]

    rot_q = turn(proj[0])
    rot_k = (turn(proj[1]) * head ** (-0.5)).astype(BF)
    vals = proj[2]
    rows = lax.broadcasted_iota(jnp.int32, (length, length), 0)
    cols = lax.broadcasted_iota(jnp.int32, (length, length), 1)
    dist = (rows - cols).astype(F32)
    lane = lax.broadcasted_iota(jnp.int32, (length, ret), 1) // head
    total = jnp.zeros((length, ret), F32)
    for h in range(heads):
        q_h = jnp.where(lane == h, rot_q, 0.0).astype(BF)
        decay = jnp.where(dist >= 0.0, jnp.exp(-forget[h] * jnp.maximum(dist, 0.0)), 0.0)
        inner = (nt(q_h, rot_k) * decay).astype(BF)
        total = jnp.where(lane == h, nn(inner, vals), total)
    mean = lax.dot_general(
        total * total, same, (((1,), (0,)), ((), ())), precision=lax.Precision.HIGHEST, preferred_element_type=F32
    )
    gate = proj[3].astype(F32)
    mixed[...] = (gate / (1.0 + jnp.exp(-gate)) * (total * lax.rsqrt(mean + 0.01))).astype(BF)

    finish(1)
    for t in range(n_tp):
        store_parts(Z, t, nt(mixed[...], full[1][t * width : (t + 1) * width, :]))
    reduce_start(Z)
    reduce_core(Z)
    relay(2)
    after = (tok[...].astype(F32) + reduce_y(Z) * out_scale).astype(BF)
    seqs[0, tp] = after

    for k in range(1, Z):
        send(seqs.at[0, tp], seqs.at[k, tp], azs.at[k - 1], azr.at[k - 1], {"fs": at_z(k)})

    def collect_z(k):
        slot = seqs.at[k, tp]
        if k:
            remote(slot, slot, azs.at[k - 1], azr.at[k - 1], {"fs": at_z(k)}).wait_recv()
        for j in range(1, Y):
            send(slot, slot, ays.at[k, j - 1], ayr.at[k, j - 1], {"tp": at_y(j)})
        for o in range(1, C):
            send(slot, slot, acs.at[k, 0, o - 1], acr.at[k, 0, o - 1], {"tp": at_core(o)})

    def collect_y(k):
        for j in range(1, Y):
            slot = seqs.at[k, at_y(Y - j)]
            remote(slot, slot, ays.at[k, j - 1], ayr.at[k, j - 1], {"tp": at_y(j)}).wait_recv()
            for o in range(1, C):
                send(slot, slot, acs.at[k, j, o - 1], acr.at[k, j, o - 1], {"tp": at_core(o)})

    def feed(k):
        for j in range(Y):
            for o in range(1, C):
                slot = seqs.at[k, lax.rem(y + Y - j, Y) * C + lax.rem(core + C - o, C)]
                remote(slot, slot, acs.at[k, j, o - 1], acr.at[k, j, o - 1], {"tp": at_core(o)}).wait_recv()
        norm(lambda t: seqs.at[k, t], 1)
        if k == 0:
            finish(2)
        chunk = hidden.shape[1]
        s = scale_row[:, pl.ds(pl.multiple_of(up_at + z * chunk, 128), chunk)]
        u = jnp.maximum(nn(normed[...], full[2][...]) * s, 0.0)
        hidden[...] = (u * u).astype(BF)
        if k == 0:
            finish(3)
        for t in range(n_tp):
            store_parts(k, t, nt(hidden[...], full[3][t * width : (t + 1) * width, :]))
        reduce_start(k)

    def give_z(k):
        value = reduce_y(k)
        z_out[k] = value.astype(BF)
        if k:
            send(z_out.at[k], z_in.at[k - 1], rzs.at[k - 1], rzr.at[k - 1], {"fs": at_z(Z - k)})

    collect_z(0)
    relay(3)
    for i in range(Z + 3):
        if 1 <= i + 1 < Z:
            collect_z(i + 1)
        if i < Z:
            collect_y(i)
        if 0 <= i - 1 < Z:
            reduce_core(i - 1)
        if 0 <= i - 2 < Z:
            give_z(i - 2)
        if i < Z:
            feed(i)
    mlp_total = z_out[0].astype(F32)
    for k in range(1, Z):
        slot = z_in.at[k - 1]
        remote(slot, slot, rzs.at[k - 1], rzr.at[k - 1], {"fs": at_z(k)}).wait_recv()
        mlp_total += z_in[k - 1].astype(F32)
    out_ref[...] = (seqs[0, tp].astype(F32) + mlp_total * down_scale).astype(BF)
    for copy in pending:
        copy.wait_send()


def tables(length, head, heads):
    half = head // 2
    inverse = 1.0 / 10000.0 ** np.linspace(0.0, 1.0, half)
    angle = np.arange(length)[:, None] * inverse.astype(np.float32).astype(np.float64)[None, :]
    spread = lambda a: np.tile(np.repeat(a, 2, axis=1), (1, heads)).astype(np.float32)
    return spread(np.cos(angle)), spread(np.sin(angle))


def solution(mesh):
    n_fs, n_tp = mesh.shape["fs"], mesh.shape["tp"]
    heights = [getattr(d, "coords", (0, 0, i))[2] for i, d in enumerate(mesh.devices[:, 0])]
    X = heights.count(heights[0])
    if n_fs % X:
        X = 1
    Z = n_fs // X
    cores = [getattr(d, "core_on_chip", 0) for d in mesh.devices[0]]
    C = len(set(cores))
    if n_tp % C:
        C = 1
    Y = n_tp // C

    def on_device(tokens, mix_gain, mlp_gain, wq, wk, wv, wg, wo, wu, wd, sq, sk, sv, sg, so, su, sd, forget):
        width, length = tokens.shape
        D = width * n_tp
        ret = wq.shape[1]
        heads = forget.shape[0]
        ff = wu.shape[1]
        chunk = ff // Z
        me = lax.axis_index("fs")

        def spot(s):
            wide = jnp.tile(s, n_fs)
            return jnp.where(jnp.arange(wide.shape[0]) // s.shape[0] == me, wide, 0.0)

        scales = jnp.concatenate([spot(s) for s in (sq, sk, sv, sg, so, sd, su)])[None, :]
        gains = jnp.stack([mix_gain, mlp_gain])
        cos_t, sin_t = tables(length, ret // heads, heads)
        own = [jnp.concatenate([w.astype(BF) for w in (wq, wk, wv, wg)], axis=1), wo.astype(BF).T]
        own.append(wu.astype(BF).reshape(-1, Z, chunk).transpose(1, 0, 2))
        own.append(wd.astype(BF).reshape(Z, chunk, -1).transpose(0, 2, 1))
        n_w = len(own)
        vm = pl.BlockSpec(memory_space=pltpu.VMEM)
        dma = pltpu.SemaphoreType.DMA
        tile = (length, width)
        scratch = [pltpu.VMEM((n_fs * w.shape[-2], w.shape[-1]), BF) for w in own]
        scratch += [
            pltpu.VMEM((n_fs,) + scales.shape, F32),
            pltpu.VMEM(scales.shape, F32),
            pltpu.VMEM((n_tp,) + tile, BF),
            pltpu.VMEM((Z, n_tp) + tile, BF),
            pltpu.VMEM((Z + 1, C, Y) + tile, BF),
            pltpu.VMEM((Z + 1, C - 1, Y) + tile, BF),
            pltpu.VMEM((Z + 1, Y) + tile, BF),
            pltpu.VMEM((Z + 1, Y - 1) + tile, BF),
            pltpu.VMEM((Z,) + tile, BF),
            pltpu.VMEM((Z - 1,) + tile, BF),
            pltpu.VMEM((length, D), BF),
            pltpu.VMEM((4, length, ret), BF),
            pltpu.VMEM((length, ret), BF),
            pltpu.VMEM((length, chunk), BF),
            dma((n_w + 2,)),
        ]
        for shape in [(n_w + 1, Z - 1), (n_w + 1, Z, X - 1), (n_tp - 1,), (Z - 1,), (Z, Y - 1), (Z, Y, C - 1),
                      (Z + 1, C - 1), (Z + 1, Y - 1), (Z - 1,)]:
            scratch += [dma(shape), dma(shape)]
        out = pl.pallas_call(
            functools.partial(kernel, (Z, X, Y, C, heads)),
            out_shape=jax.ShapeDtypeStruct((length, width), BF),
            in_specs=[vm] * 5 + [pl.BlockSpec(memory_space=pltpu.SMEM)] + [vm] * n_w,
            out_specs=vm,
            scratch_shapes=scratch,
            compiler_params=pltpu.CompilerParams(
                collective_id=0, has_side_effects=True, vmem_limit_bytes=60 * 2**20
            ),
            name="layer",
        )(tokens.T, gains, scales, jnp.asarray(cos_t), jnp.asarray(sin_t), forget, *own)
        return out.T

    cut = P(("tp", "fs"))
    rows, cols = P("fs", "tp"), P("tp", "fs")
    in_specs = (cols, P(), P(), rows, rows, rows, rows, cols, rows, cols) + (cut,) * 7 + (P("tp"),)
    return jax.shard_map(on_device, mesh=mesh, in_specs=in_specs, out_specs=cols, check_vma=False)
```

time: 327 us -> 240 us (0.73)
  the two profiles are of different devices: /device:TPU:9 before, /device:TPU:0 now
where the time goes in v2:
time: 240 us; the launch traced here: 239 us
  Pallas kernels  225 us (94%)
  local copies, waits for them, and re-layouts  12.6 us (5%)
    pallas_call x1, Pallas kernels, on_device(): pl.pallas_call(functools.partial(kernel, (Z, X, Y, C, heads)), out_shape=...  225 us

profile of v2, /device:TPU:0, one launch (start us, length us, event | category | flops | bytes accessed | tf_op | source)
XLA Modules:
  0.0 239.4 jit_solution(18393675829137812741)
XLA Ops:
  0.0 0.0 copy-start
  0.0 0.7 tile.28
  0.7 0.1 tile.29
  0.8 0.7 tile.30
  1.4 0.1 tile.31
  1.5 0.7 tile.32
  2.2 0.1 tile.33
  2.3 0.7 tile.34
  2.9 0.1 tile.70
  3.0 0.7 tile.71
  3.7 0.1 tile.72
  3.8 0.7 tile.73
  4.4 0.1 tile.74
  4.5 0.0 copy-done
  4.5 0.0 copy-start.8
  4.5 0.0 copy-start.1
  4.6 1.9 copy.26
  6.5 1.3 copy.27
  7.8 0.0 copy-done.8
  7.8 0.0 copy-done.1
  7.8 0.0 copy-start.3
  7.8 0.1 convert_element_type.27
  7.9 0.0 copy-start.4
  7.9 0.0 copy-start.5
  7.9 0.0 copy-start.6
  7.9 0.0 copy-start.2
  8.0 1.3 copy.28
  9.3 0.0 copy-start.7
  9.3 0.0 copy-start.9
  9.3 0.0 copy-start.10
  9.3 0.0 copy-done.3
  9.3 0.0 copy-done.4
  9.3 0.0 copy-done.5
  9.4 0.0 copy-done.6
  9.4 0.9 pad_maximum_fusion.refs_6_
  10.3 0.0 copy-done.2
  10.3 0.9 copy.24
  11.2 0.0 copy-done.7
  11.2 0.8 copy.25
  12.0 0.0 copy-done.9
  12.0 0.0 copy-done.10
  12.0 0.6 pad_maximum_fusion.1.refs_1_
  12.6 224.9 %layer.1 = bf16[384,512]{1,0:T(8,128)(2,1)} custom-call(bf16[384,512]{1,0:T(8,128)(2,1)} %bitcast.20, f32[2,2048]{1,0:T(2,128)} %pad_maximum_fusion.1.refs_1_, f32[1,4096]{1,0:T(1,128)} %bitcast.23, f32[384,256]{1,0:T(8,128)} %constant.68.clone.refs_3_, f32[384,256]{1,0:T(8,128)} %constant.69.clone.refs_4_, f32[4]{0:T(128)} %refs_5_.1, ...), custom_call_target="tpu_custom_call" | custom-call | tf_op jit(solution)/shard_map/layer/pallas_call | solution.py:357
  237.5 1.9 copy.29
  (14 shorter events, 0.1 us)
Async XLA Ops:
  0.0 4.5 %copy-start = (f32[256]{0:T(256)S(1)}, f32[256]{0:T(256)}, u32[]{:S(2)}) copy-start(f32[256]{0:T(256)} %param.35) | copy-start | bytes 3076
  4.5 3.3 %copy-start.8 = (f32[4096]{0:T(1024)}, f32[4096]{0:T(1024)S(1)}, u32[]{:S(2)}) copy-start(f32[4096]{0:T(1024)S(1)} %select_dynamic-update-slice_fusion) | copy-start | bytes 49156
  4.5 3.2 %copy-start.1 = (f32[2048,256]{1,0:T(8,128)S(1)}, f32[2048,256]{1,0:T(8,128)}, u32[]{:S(2)}) copy-start(f32[2048,256]{1,0:T(8,128)} %param.29) | copy-start | bytes 6291460
  7.8 1.5 copy-start.3
  7.9 1.4 copy-start.4
  7.9 1.4 copy-start.5
  7.9 1.5 copy-start.6
  7.9 2.4 copy-start.2
  9.3 2.0 copy-start.7
  9.3 2.7 %copy-start.9 = (f32[2048]{0:T(1024)S(1)}, f32[2048]{0:T(1024)}, u32[]{:S(2)}) copy-start(f32[2048]{0:T(1024)} %param.22) | copy-start | bytes 24580
  9.3 2.7 %copy-start.10 = (f32[2048]{0:T(1024)S(1)}, f32[2048]{0:T(1024)}, u32[]{:S(2)}) copy-start(f32[2048]{0:T(1024)} %param.21) | copy-start | bytes 24580

commit v3 on v2

--- a/solution.py
+++ b/solution.py
@@ -22,7 +22,7 @@
 
 
 def kernel(cfg, *refs):
-    Z, X, Y, C, heads = cfg
+    Z, X, Y, C, G, heads = cfg
     n_tp = Y * C
     n_w = 4
     tok, gains, scales, cos_t, sin_t, forget = refs[:6]
@@ -45,6 +45,9 @@
     def at_z(o):
         return lax.rem(z + o, Z) * X + x
 
+    def at_g(o):
+        return (z // G * G + lax.rem(z + o, G)) * X + x
+
     def at_x(o):
         return z * X + lax.rem(x + o, X)
 
@@ -87,7 +90,7 @@
     def mine(w, o):
         if w == n_w:
             return scales
-        return own[w].at[lax.rem(z + o, Z)] if w >= 2 else own[w]
+        return own[w].at[lax.rem(z + o, G)] if w >= 2 else own[w]
 
     def z_send(w):
         for o in range(1, Z):
@@ -156,7 +159,6 @@
         z_send(w)
         x_own(w)
     z_send(2)
-    z_send(3)
     locals_ = [pltpu.make_async_copy(mine(w, 0), place(w, me), local_sem.at[w]) for w in range(n_w + 1)]
     locals_.append(pltpu.make_async_copy(tok, tok_g.at[tp], local_sem.at[n_w + 1]))
     for copy in locals_:
@@ -216,20 +218,20 @@
 
     finish(1)
     for t in range(n_tp):
-        store_parts(Z, t, nt(mixed[...], full[1][t * width : (t + 1) * width, :]))
-    reduce_start(Z)
-    reduce_core(Z)
-    relay(2)
-    after = (tok[...].astype(F32) + reduce_y(Z) * out_scale).astype(BF)
+        store_parts(G, t, nt(mixed[...], full[1][t * width : (t + 1) * width, :]))
+    reduce_start(G)
+    reduce_core(G)
+    after = (tok[...].astype(F32) + reduce_y(G) * out_scale).astype(BF)
     seqs[0, tp] = after
 
-    for k in range(1, Z):
-        send(seqs.at[0, tp], seqs.at[k, tp], azs.at[k - 1], azr.at[k - 1], {"fs": at_z(k)})
+    for k in range(1, G):
+        send(seqs.at[0, tp], seqs.at[k, tp], azs.at[k - 1], azr.at[k - 1], {"fs": at_g(k)})
+    z_send(3)
 
     def collect_z(k):
         slot = seqs.at[k, tp]
         if k:
-            remote(slot, slot, azs.at[k - 1], azr.at[k - 1], {"fs": at_z(k)}).wait_recv()
+            remote(slot, slot, azs.at[k - 1], azr.at[k - 1], {"fs": at_g(k)}).wait_recv()
         for j in range(1, Y):
             send(slot, slot, ays.at[k, j - 1], ayr.at[k, j - 1], {"tp": at_y(j)})
         for o in range(1, C):
@@ -248,41 +250,56 @@
                 slot = seqs.at[k, lax.rem(y + Y - j, Y) * C + lax.rem(core + C - o, C)]
                 remote(slot, slot, acs.at[k, j, o - 1], acr.at[k, j, o - 1], {"tp": at_core(o)}).wait_recv()
         norm(lambda t: seqs.at[k, t], 1)
-        if k == 0:
-            finish(2)
-        chunk = hidden.shape[1]
-        s = scale_row[:, pl.ds(pl.multiple_of(up_at + z * chunk, 128), chunk)]
-        u = jnp.maximum(nn(normed[...], full[2][...]) * s, 0.0)
-        hidden[...] = (u * u).astype(BF)
-        if k == 0:
-            finish(3)
+
+    def expand(k):
+        chunk = hidden.shape[2]
+        step = 256 if chunk % 256 == 0 else chunk
+
+        def tile(i, carry):
+            here = pl.ds(pl.multiple_of(i * step, step), step)
+            s = scale_row[:, pl.ds(pl.multiple_of(up_at + lax.rem(z, G) * chunk + i * step, 128), step)]
+            u = jnp.maximum(nn(normed[...], full[2][:, here]) * s, 0.0)
+            hidden[k, :, here] = (u * u).astype(BF)
+            return carry
+
+        lax.fori_loop(0, chunk // step, tile, 0)
+
+    def shrink(k):
         for t in range(n_tp):
-            store_parts(k, t, nt(hidden[...], full[3][t * width : (t + 1) * width, :]))
+            store_parts(k, t, nt(hidden[k], full[3][t * width : (t + 1) * width, :]))
         reduce_start(k)
 
     def give_z(k):
         value = reduce_y(k)
         z_out[k] = value.astype(BF)
         if k:
-            send(z_out.at[k], z_in.at[k - 1], rzs.at[k - 1], rzr.at[k - 1], {"fs": at_z(Z - k)})
+            send(z_out.at[k], z_in.at[k - 1], rzs.at[k - 1], rzr.at[k - 1], {"fs": at_g(G - k)})
 
     collect_z(0)
+    relay(2)
+    for k in range(1, G):
+        collect_z(k)
+    collect_y(0)
+    feed(0)
+    finish(2)
+    expand(0)
+    for k in range(1, G):
+        collect_y(k)
+        feed(k)
+        expand(k)
     relay(3)
-    for i in range(Z + 3):
-        if 1 <= i + 1 < Z:
-            collect_z(i + 1)
-        if i < Z:
-            collect_y(i)
-        if 0 <= i - 1 < Z:
-            reduce_core(i - 1)
-        if 0 <= i - 2 < Z:
-            give_z(i - 2)
-        if i < Z:
-            feed(i)
+    finish(3)
+    order = list(range(1, G)) + [0]
+    for k in order:
+        shrink(k)
+    for k in order:
+        reduce_core(k)
+    for k in order:
+        give_z(k)
     mlp_total = z_out[0].astype(F32)
-    for k in range(1, Z):
+    for k in range(1, G):
         slot = z_in.at[k - 1]
-        remote(slot, slot, rzs.at[k - 1], rzr.at[k - 1], {"fs": at_z(k)}).wait_recv()
+        remote(slot, slot, rzs.at[k - 1], rzr.at[k - 1], {"fs": at_g(k)}).wait_recv()
         mlp_total += z_in[k - 1].astype(F32)
     out_ref[...] = (seqs[0, tp].astype(F32) + mlp_total * down_scale).astype(BF)
     for copy in pending:
@@ -309,6 +326,7 @@
     if n_tp % C:
         C = 1
     Y = n_tp // C
+    G = 2 if Z % 2 == 0 else Z
 
     def on_device(tokens, mix_gain, mlp_gain, wq, wk, wv, wg, wo, wu, wd, sq, sk, sv, sg, so, su, sd, forget):
         width, length = tokens.shape
@@ -316,7 +334,7 @@
         ret = wq.shape[1]
         heads = forget.shape[0]
         ff = wu.shape[1]
-        chunk = ff // Z
+        chunk = ff // G
         me = lax.axis_index("fs")
 
         def spot(s):
@@ -327,8 +345,8 @@
         gains = jnp.stack([mix_gain, mlp_gain])
         cos_t, sin_t = tables(length, ret // heads, heads)
         own = [jnp.concatenate([w.astype(BF) for w in (wq, wk, wv, wg)], axis=1), wo.astype(BF).T]
-        own.append(wu.astype(BF).reshape(-1, Z, chunk).transpose(1, 0, 2))
-        own.append(wd.astype(BF).reshape(Z, chunk, -1).transpose(0, 2, 1))
+        own.append(wu.astype(BF).reshape(-1, G, chunk).transpose(1, 0, 2))
+        own.append(wd.astype(BF).reshape(G, chunk, -1).transpose(0, 2, 1))
         n_w = len(own)
         vm = pl.BlockSpec(memory_space=pltpu.VMEM)
         dma = pltpu.SemaphoreType.DMA
@@ -338,24 +356,24 @@
             pltpu.VMEM((n_fs,) + scales.shape, F32),
             pltpu.VMEM(scales.shape, F32),
             pltpu.VMEM((n_tp,) + tile, BF),
-            pltpu.VMEM((Z, n_tp) + tile, BF),
-            pltpu.VMEM((Z + 1, C, Y) + tile, BF),
-            pltpu.VMEM((Z + 1, C - 1, Y) + tile, BF),
-            pltpu.VMEM((Z + 1, Y) + tile, BF),
-            pltpu.VMEM((Z + 1, Y - 1) + tile, BF),
-            pltpu.VMEM((Z,) + tile, BF),
-            pltpu.VMEM((Z - 1,) + tile, BF),
+            pltpu.VMEM((G, n_tp) + tile, BF),
+            pltpu.VMEM((G + 1, C, Y) + tile, BF),
+            pltpu.VMEM((G + 1, C - 1, Y) + tile, BF),
+            pltpu.VMEM((G + 1, Y) + tile, BF),
+            pltpu.VMEM((G + 1, Y - 1) + tile, BF),
+            pltpu.VMEM((G,) + tile, BF),
+            pltpu.VMEM((G - 1,) + tile, BF),
             pltpu.VMEM((length, D), BF),
             pltpu.VMEM((4, length, ret), BF),
             pltpu.VMEM((length, ret), BF),
-            pltpu.VMEM((length, chunk), BF),
+            pltpu.VMEM((G, length, chunk), BF),
             dma((n_w + 2,)),
         ]
-        for shape in [(n_w + 1, Z - 1), (n_w + 1, Z, X - 1), (n_tp - 1,), (Z - 1,), (Z, Y - 1), (Z, Y, C - 1),
-                      (Z + 1, C - 1), (Z + 1, Y - 1), (Z - 1,)]:
+        for shape in [(n_w + 1, Z - 1), (n_w + 1, Z, X - 1), (n_tp - 1,), (G - 1,), (G, Y - 1), (G, Y, C - 1),
+                      (G + 1, C - 1), (G + 1, Y - 1), (G - 1,)]:
             scratch += [dma(shape), dma(shape)]
         out = pl.pallas_call(
-            functools.partial(kernel, (Z, X, Y, C, heads)),
+            functools.partial(kernel, (Z, X, Y, C, G, heads)),
             out_shape=jax.ShapeDtypeStruct((length, width), BF),
             in_specs=[vm] * 5 + [pl.BlockSpec(memory_space=pltpu.SMEM)] + [vm] * n_w,
             out_specs=vm,

time: 240 us -> 242 us (level)
  no operation moved by 1% of the time
where the time goes in v3:
time: 242 us
  Pallas kernels  227 us (94%)
  local copies, waits for them, and re-layouts  12.6 us (5%)
    pallas_call x1, Pallas kernels, on_device(): pl.pallas_call(functools.partial(kernel, (Z, X, Y, C, G, heads)), out_sha...  227 us

profile of v3, /device:TPU:0, one launch (start us, length us, event | category | flops | bytes accessed | tf_op | source)
XLA Modules:
  0.0 241.8 jit_solution(18401422316657651077)
XLA Ops:
  0.0 0.0 copy-start
  0.0 0.7 tile.28
  0.7 0.1 tile.29
  0.8 0.7 tile.30
  1.4 0.1 tile.31
  1.5 0.7 tile.32
  2.2 0.1 tile.33
  2.3 0.7 tile.34
  2.9 0.1 tile.70
  3.0 0.7 tile.71
  3.7 0.1 tile.72
  3.8 0.7 tile.73
  4.4 0.1 tile.74
  4.5 0.0 copy-done
  4.5 0.0 copy-start.8
  4.5 0.0 copy-start.1
  4.6 1.9 copy.26
  6.5 1.3 copy.27
  7.8 0.0 copy-done.8
  7.8 0.0 copy-done.1
  7.8 0.0 copy-start.3
  7.8 0.1 convert_element_type.27
  7.9 0.0 copy-start.4
  7.9 0.0 copy-start.5
  7.9 0.0 copy-start.6
  7.9 0.0 copy-start.2
  7.9 1.3 copy.28
  9.3 0.0 copy-start.7
  9.3 0.0 copy-start.9
  9.3 0.0 copy-start.10
  9.3 0.0 copy-done.3
  9.3 0.0 copy-done.4
  9.3 0.0 copy-done.5
  9.4 0.0 copy-done.6
  9.4 0.9 pad_maximum_fusion.refs_6_
  10.3 0.0 copy-done.2
  10.3 0.9 copy.24
  11.2 0.0 copy-done.7
  11.2 0.8 copy.25
  12.0 0.0 copy-done.9
  12.0 0.0 copy-done.10
  12.0 0.6 pad_maximum_fusion.1.refs_1_
  12.6 227.3 %layer.1 = bf16[384,512]{1,0:T(8,128)(2,1)} custom-call(bf16[384,512]{1,0:T(8,128)(2,1)} %bitcast.20, f32[2,2048]{1,0:T(2,128)} %pad_maximum_fusion.1.refs_1_, f32[1,4096]{1,0:T(1,128)} %bitcast.23, f32[384,256]{1,0:T(8,128)} %constant.68.clone.refs_3_, f32[384,256]{1,0:T(8,128)} %constant.69.clone.refs_4_, f32[4]{0:T(128)} %refs_5_.1, ...), custom_call_target="tpu_custom_call" | custom-call | tf_op jit(solution)/shard_map/layer/pallas_call | solution.py:375
  239.9 1.9 copy.29
  (14 shorter events, 0.1 us)
Async XLA Ops:
  0.0 4.5 %copy-start = (f32[256]{0:T(256)S(1)}, f32[256]{0:T(256)}, u32[]{:S(2)}) copy-start(f32[256]{0:T(256)} %param.35) | copy-start | bytes 3076
  4.5 3.2 %copy-start.8 = (f32[4096]{0:T(1024)}, f32[4096]{0:T(1024)S(1)}, u32[]{:S(2)}) copy-start(f32[4096]{0:T(1024)S(1)} %select_dynamic-update-slice_fusion) | copy-start | bytes 49156
  4.5 3.2 %copy-start.1 = (f32[2048,256]{1,0:T(8,128)S(1)}, f32[2048,256]{1,0:T(8,128)}, u32[]{:S(2)}) copy-start(f32[2048,256]{1,0:T(8,128)} %param.29) | copy-start | bytes 6291460
  7.8 1.5 copy-start.3
  7.9 1.4 copy-start.4
  7.9 1.4 copy-start.5
  7.9 1.5 copy-start.6
  7.9 2.3 copy-start.2
  9.3 2.0 copy-start.7
  9.3 2.7 %copy-start.9 = (f32[2048]{0:T(1024)S(1)}, f32[2048]{0:T(1024)}, u32[]{:S(2)}) copy-start(f32[2048]{0:T(1024)} %param.22) | copy-start | bytes 24580
  9.3 2.7 %copy-start.10 = (f32[2048]{0:T(1024)S(1)}, f32[2048]{0:T(1024)}, u32[]{:S(2)}) copy-start(f32[2048]{0:T(1024)} %param.21) | copy-start | bytes 24580

commit v4 on v3

--- a/solution.py
+++ b/solution.py
@@ -158,7 +158,6 @@
     for w in (n_w, 0, 1):
         z_send(w)
         x_own(w)
-    z_send(2)
     locals_ = [pltpu.make_async_copy(mine(w, 0), place(w, me), local_sem.at[w]) for w in range(n_w + 1)]
     locals_.append(pltpu.make_async_copy(tok, tok_g.at[tp], local_sem.at[n_w + 1]))
     for copy in locals_:
@@ -173,10 +172,10 @@
     relay(n_w)
     relay(0)
     relay(1)
-    x_own(2)
-    x_own(3)
+    z_send(2)
     finish(n_w)
     finish(0)
+    x_own(2)
     scale = jnp.sum(scale_g[...], axis=0)
     scale_row[...] = scale
     at = 4 * ret
@@ -217,6 +216,7 @@
     mixed[...] = (gate / (1.0 + jnp.exp(-gate)) * (total * lax.rsqrt(mean + 0.01))).astype(BF)
 
     finish(1)
+    x_own(3)
     for t in range(n_tp):
         store_parts(G, t, nt(mixed[...], full[1][t * width : (t + 1) * width, :]))
     reduce_start(G)
@@ -226,7 +226,6 @@
 
     for k in range(1, G):
         send(seqs.at[0, tp], seqs.at[k, tp], azs.at[k - 1], azr.at[k - 1], {"fs": at_g(k)})
-    z_send(3)
 
     def collect_z(k):
         slot = seqs.at[k, tp]
@@ -279,6 +278,7 @@
     relay(2)
     for k in range(1, G):
         collect_z(k)
+    z_send(3)
     collect_y(0)
     feed(0)
     finish(2)

time: 242 us -> 229 us (0.946)
  the two profiles are of different devices: /device:TPU:0 before, /device:TPU:16 now
where the time goes in v4:
time: 229 us
  Pallas kernels  214 us (93%)
  local copies, waits for them, and re-layouts  12.6 us (6%)
    pallas_call x1, Pallas kernels, on_device(): pl.pallas_call(functools.partial(kernel, (Z, X, Y, C, G, heads)), out_sha...  214 us

profile of v4, /device:TPU:16, one launch (start us, length us, event | category | flops | bytes accessed | tf_op | source)
XLA Modules:
  0.0 228.7 jit_solution(13369882979731693289)
XLA Ops:
  0.0 0.0 copy-start
  0.0 0.7 tile.28
  0.7 0.1 tile.29
  0.8 0.7 tile.30
  1.4 0.1 tile.31
  1.5 0.7 tile.32
  2.2 0.1 tile.33
  2.3 0.7 tile.34
  2.9 0.1 tile.70
  3.0 0.7 tile.71
  3.7 0.1 tile.72
  3.8 0.7 tile.73
  4.4 0.1 tile.74
  4.5 0.0 copy-done
  4.5 0.0 copy-start.8
  4.5 0.0 copy-start.1
  4.6 1.9 copy.26
  6.5 1.3 copy.27
  7.8 0.0 copy-done.8
  7.8 0.0 copy-done.1
  7.8 0.0 copy-start.3
  7.8 0.1 convert_element_type.27
  7.9 0.0 copy-start.4
  7.9 0.0 copy-start.5
  7.9 0.0 copy-start.6
  7.9 0.0 copy-start.2
  7.9 1.3 copy.28
  9.3 0.0 copy-start.7
  9.3 0.0 copy-start.9
  9.3 0.0 copy-start.10
  9.3 0.0 copy-done.3
  9.3 0.0 copy-done.4
  9.3 0.0 copy-done.5
  9.4 0.0 copy-done.6
  9.4 0.9 pad_maximum_fusion.refs_6_
  10.3 0.0 copy-done.2
  10.3 0.9 copy.24
  11.2 0.0 copy-done.7
  11.2 0.8 copy.25
  12.0 0.0 copy-done.9
  12.0 0.0 copy-done.10
  12.0 0.6 pad_maximum_fusion.1.refs_1_
  12.6 214.2 %layer.1 = bf16[384,512]{1,0:T(8,128)(2,1)} custom-call(bf16[384,512]{1,0:T(8,128)(2,1)} %bitcast.20, f32[2,2048]{1,0:T(2,128)} %pad_maximum_fusion.1.refs_1_, f32[1,4096]{1,0:T(1,128)} %bitcast.23, f32[384,256]{1,0:T(8,128)} %constant.68.clone.refs_3_, f32[384,256]{1,0:T(8,128)} %constant.69.clone.refs_4_, f32[4]{0:T(128)} %refs_5_.1, ...), custom_call_target="tpu_custom_call" | custom-call | tf_op jit(solution)/shard_map/layer/pallas_call | solution.py:375
  226.8 1.9 copy.29
  (14 shorter events, 0.1 us)
Async XLA Ops:
  0.0 4.5 %copy-start = (f32[256]{0:T(256)S(1)}, f32[256]{0:T(256)}, u32[]{:S(2)}) copy-start(f32[256]{0:T(256)} %param.35) | copy-start | bytes 3076
  4.5 3.2 %copy-start.8 = (f32[4096]{0:T(1024)}, f32[4096]{0:T(1024)S(1)}, u32[]{:S(2)}) copy-start(f32[4096]{0:T(1024)S(1)} %select_dynamic-update-slice_fusion) | copy-start | bytes 49156
  4.5 3.2 %copy-start.1 = (f32[2048,256]{1,0:T(8,128)S(1)}, f32[2048,256]{1,0:T(8,128)}, u32[]{:S(2)}) copy-start(f32[2048,256]{1,0:T(8,128)} %param.29) | copy-start | bytes 6291460
  7.8 1.5 copy-start.3
  7.9 1.4 copy-start.4
  7.9 1.4 copy-start.5
  7.9 1.5 copy-start.6
  7.9 2.3 %copy-start.2 = (bf16[512,384]{1,0:T(8,128)(2,1)S(1)}, bf16[512,384]{1,0:T(8,128)(2,1)}, u32[]{:S(2)}) copy-start(bf16[512,384]{1,0:T(8,128)(2,1)} %param.20) | copy-start | bytes 1179652
  9.3 2.0 copy-start.7
  9.3 2.7 %copy-start.9 = (f32[2048]{0:T(1024)S(1)}, f32[2048]{0:T(1024)}, u32[]{:S(2)}) copy-start(f32[2048]{0:T(1024)} %param.22) | copy-start | bytes 24580
  9.3 2.7 %copy-start.10 = (f32[2048]{0:T(1024)S(1)}, f32[2048]{0:T(1024)}, u32[]{:S(2)}) copy-start(f32[2048]{0:T(1024)} %param.21) | copy-start | bytes 24580
